TPU v7x, 32 devices: a whole 2x2x4 slice. The times are simulated.
32 devices in a mesh: sp: 4 (over z), fs: 4 (over y, x), tp: 2 (over core).
Axes of the slice: x: 2, y: 2, z: 4, core: 2. Of those that a mesh axis runs over, the one named last changes fastest.
Arguments:
- tokens: bfloat16 [4, 512, 2048], P('fs', ('sp', 'tp')), may hold values from -6 to 6
- input_norm_gain: float32 [2048], replicated, may hold values from 0.1 to 1.9
- pooling_input_weight: bfloat16 [2048, 1024], P('sp', 'tp'), may hold values from -0.125 to 0.125
- query_weight: bfloat16 [2048, 1024], P('sp', 'tp'), may hold values from -0.125 to 0.125
- forget_weight: bfloat16 [2048, 1024], P('sp', 'tp'), may hold values from -0.125 to 0.125
- value_weight: bfloat16 [2048, 1024], P('sp', 'tp'), may hold values from -0.125 to 0.125
- pooling_group_maps: bfloat16 [4, 256, 256], P('tp'), may hold values from -0.375 to 0.375
- pooling_scale: float32 [1024], P('tp'), may hold values from 0.1 to 1.9
- lower_bound_logits: float32 [1024], P('tp')
- decay_spike: float32 [4, 512, 8], P('fs', 'sp', 'tp'), may hold values from -0.75 to 0
- head_norm_gain: float32 [1024], P('tp'), may hold values from 0.1 to 1.9
- pooling_output_weight: bfloat16 [1024, 2048], P('tp', 'sp'), may hold values from -0.125 to 0.125
- recurrent_output_weight: bfloat16 [1024, 2048], P('tp', 'sp'), may hold values from -0.125 to 0.125
Outputs:
- mixed: bfloat16 [4, 512, 2048], P('fs', ('sp', 'tp'))
All inputs are finite; a program needn't handle non-finite values.
Results may differ from a plain program's by a relative error of at most 0.013.
Values may be sent and summed in bfloat16 or wider, within the bound.
A program may use at most 64 MiB of HBM per device.

v0:
```python
import jax
import jax.numpy as jnp
from jax import lax
from jax.sharding import PartitionSpec as P

BLOCK = 64


EPSILON = 1e-06
HIGHEST = lax.Precision.HIGHEST


def shifted(value, axis, steps):
    count = lax.axis_size(axis)
    first, last = (max(0, -steps), min(count, count - steps))
    return lax.ppermute(value, axis, [(source, source + steps) for source in range(first, last)])


def entering(shard, axis, join, neutral):
    place = lax.axis_index(axis)
    gathered = jax.tree.map(
        lambda a, kind: lax.all_gather(a.astype(kind), axis), shard, (jnp.bfloat16, jnp.bfloat16)
    )
    state = jax.tree.map(lambda a, e: jnp.zeros_like(a) + jnp.asarray(e, a.dtype), shard, neutral)

    def one(step, state):
        return join(
            state,
            jax.tree.map(
                lambda a, own: lax.dynamic_index_in_dim(a, step, 0, False).astype(own.dtype),
                gathered,
                shard,
            ),
        )

    return lax.fori_loop(0, place, one, state)


def rms_scale(values, gain):
    return values * lax.rsqrt(jnp.mean(values * values, axis=-1, keepdims=True) + EPSILON) * gain


def join_state(earlier, later):
    decay_one, state_one = earlier
    decay_two, state_two = later
    return (decay_one * decay_two, decay_two[..., None] * state_one + state_two)


def body(
    tokens,
    input_norm_gain,
    pooling_input_weight,
    query_weight,
    forget_weight,
    value_weight,
    pooling_group_maps,
    pooling_scale,
    lower_bound_logits,
    decay_spike,
    head_norm_gain,
    pooling_output_weight,
    recurrent_output_weight,
):
    gathered = lax.all_gather(tokens, "tp", axis=1, tiled=True)[0]
    length_total = gathered.shape[0]
    normed = rms_scale(gathered.astype(jnp.float32), input_norm_gain).astype(jnp.bfloat16)
    pool_width = pooling_input_weight.shape[1]
    rec_width = query_weight.shape[1]
    stacked = jnp.concatenate(
        [pooling_input_weight, query_weight, forget_weight, value_weight], axis=1
    )
    out_local = jnp.concatenate([pooling_output_weight, recurrent_output_weight], axis=0)
    groups_fs = lax.axis_size("fs")
    member = lax.axis_index("fs")
    slice_width = stacked.shape[1] // groups_fs
    own_slice = lax.dynamic_slice_in_dim(stacked, member * slice_width, slice_width, 1)
    column_part = lax.all_gather(own_slice, "sp", axis=0, tiled=True)
    full_input = lax.all_gather(column_part, "fs", axis=1, tiled=True)
    projected = jnp.dot(normed, full_input, preferred_element_type=jnp.float32)
    slice_height = out_local.shape[0] // groups_fs
    own_rows = lax.dynamic_slice_in_dim(out_local, member * slice_height, slice_height, 0)
    row_part = lax.all_gather(own_rows, "sp", axis=1, tiled=True)
    out_full = lax.all_gather(row_part, "fs", axis=0, tiled=True)
    rounded = lax.optimization_barrier(projected.astype(jnp.bfloat16))
    pool_input = rounded[:, :pool_width]
    query_matrix = rounded[:, pool_width : pool_width + rec_width].astype(jnp.float32)
    forget_gate_logit = rounded[:, pool_width + rec_width : pool_width + 2 * rec_width].astype(
        jnp.float32
    )
    value_projected = rounded[:, pool_width + 2 * rec_width :].astype(jnp.float32)
    groups_local = pooling_group_maps.shape[0]
    group_size = pooling_group_maps.shape[1]
    reach_rows = 2 ** (groups_local * lax.axis_size("tp"))
    previous = shifted(pool_input[length_total - reach_rows :], "sp", 1)
    extended = jnp.concatenate([previous, pool_input], axis=0).astype(jnp.float32)
    extended = extended.reshape(reach_rows + length_total, groups_local, group_size)
    group_ids = lax.axis_index("tp") * groups_local + jnp.arange(groups_local, dtype=jnp.int32)
    windows = jnp.left_shift(jnp.int32(2), group_ids)
    window_sum = jnp.zeros((length_total, groups_local, group_size), jnp.float32)
    for offset in range(reach_rows):
        inside = (offset < windows).astype(jnp.float32)
        window_sum = (
            window_sum
            + extended[reach_rows - offset : reach_rows - offset + length_total] * inside[:, None]
        )
    position_index = lax.axis_index("sp") * length_total + jnp.arange(length_total, dtype=jnp.int32)
    counts = jnp.minimum(position_index[:, None] + 1, windows[None, :]).astype(jnp.float32)
    pool_diff = (window_sum / counts[:, :, None] - extended[reach_rows:]).astype(jnp.bfloat16)
    pool_mapped = jnp.einsum(
        "tgc,gcd->tgd", pool_diff, pooling_group_maps, preferred_element_type=jnp.float32
    )
    pool_out = (pool_mapped.reshape(length_total, pool_width) * pooling_scale).astype(jnp.bfloat16)
    local_heads = decay_spike.shape[2]
    head_width = rec_width // local_heads
    blocks = length_total // BLOCK
    block_layout = (blocks, BLOCK, local_heads, head_width)
    reader = jax.nn.silu(query_matrix).reshape(block_layout)
    key_gate_value = jax.nn.sigmoid(-lower_bound_logits) * jax.nn.sigmoid(-forget_gate_logit)
    decay_logarithm = (
        jnp.log1p(-key_gate_value).reshape(length_total, local_heads, head_width)
        + decay_spike[0][:, :, None]
    ).reshape(block_layout)
    key_rows = key_gate_value.reshape(block_layout)
    value_rows = value_projected.reshape(block_layout)
    inner_log = jnp.cumsum(decay_logarithm, axis=1)
    read_scaled = reader * jnp.exp(inner_log)
    key_scaled = key_rows * jnp.exp(-inner_log)
    causal = (jnp.arange(BLOCK)[:, None] >= jnp.arange(BLOCK)[None, :]).astype(jnp.float32)
    scores = jnp.einsum("nthd,nshd->nhts", read_scaled, key_scaled, precision=HIGHEST) * causal
    within = jnp.einsum("nhts,nshe->nthe", scores, value_rows, precision=HIGHEST)
    closing = inner_log[:, -1]
    key_tail = key_rows * jnp.exp(closing[:, None] - inner_log)
    deltas = jnp.einsum("nshd,nshe->nhde", key_tail, value_rows, precision=HIGHEST)
    block_decay = jnp.exp(closing)

    def advance(carried, input_batch):
        decay_now, delta_now = input_batch
        return (decay_now[..., None] * carried + delta_now, carried)

    initial = jnp.zeros((local_heads, head_width, head_width), jnp.float32)
    device_state, entry_states = lax.scan(advance, initial, (block_decay, deltas))
    device_decay = jnp.exp(jnp.sum(closing, axis=0))
    scanned = entering(
        (device_decay, device_state),
        "sp",
        join_state,
        (jnp.ones_like(device_decay), jnp.zeros_like(device_state)),
    )
    prior_state = scanned[1]
    before = jnp.cumsum(closing, axis=0) - closing
    start_states = entry_states + jnp.exp(before)[..., None] * prior_state[None]
    read_out = within + jnp.einsum("nthd,nhde->nthe", read_scaled, start_states, precision=HIGHEST)
    read_out = read_out.reshape(length_total, local_heads, head_width)
    recurrent_output = (
        rms_scale(read_out, 1.0).reshape(length_total, rec_width) * head_norm_gain
    ).astype(jnp.bfloat16)
    mixed_rows = jnp.concatenate([pool_out, recurrent_output], axis=1)
    summed = lax.psum_scatter(
        jnp.dot(mixed_rows, out_full, preferred_element_type=jnp.float32).astype(jnp.bfloat16),
        "tp",
        scatter_dimension=0,
        tiled=True,
    )
    return summed[None]


def solution(mesh):
    placed = (
        P("fs", ("sp", "tp"), None),
        P(),
        P("sp", "tp"),
        P("sp", "tp"),
        P("sp", "tp"),
        P("sp", "tp"),
        P("tp", None, None),
        P("tp"),
        P("tp"),
        P("fs", "sp", "tp"),
        P("tp"),
        P("tp", "sp"),
        P("tp", "sp"),
    )
    return jax.shard_map(
        body, mesh=mesh, in_specs=placed, out_specs=P("fs", ("sp", "tp"), None), check_vma=False
    )
```

profile of v0, /device:TPU:0, one launch (start us, length us, event | category | flops | bytes accessed | tf_op | source)
XLA Modules:
  0.0 247.2 jit_solution(11630460486678041191)
XLA Ops:
  6.5 0.0 all-gather.8.cloned.1.call-start
  6.6 2.3 fusion.8
  8.9 0.0 all-gather.8.cloned.1.call-update
  8.9 0.0 all-gather.12.cloned.1.call-start
  9.0 1.8 fusion.17
  10.8 0.0 all-gather.12.cloned.1.call-update
  10.9 0.0 all-gather.10.cloned.1.call-start
  10.9 46.6 %all-gather.8.cloned.1.call-done = bf16[2048,512]{1,0:T(8,128)(2,1)} async-done(((bf16[512,512]{1,0:T(8,128)(2,1)}), bf16[2048,512]{1,0:T(8,128)(2,1)}) %all-gather.8.cloned.1.call-update) | async-done | bytes 2097168 | tf_op jit(solution)/shard_map/all_gather | solution.py:77
  57.5 0.0 all-gather.10.cloned.1.call-update
  57.5 0.0 all-gather.14.cloned.1.call-start
  57.6 0.1 copy.116
  57.9 2.2 all_gather.25
  60.1 0.2 fusion.2
  60.3 0.1 minimum_convert_fusion
  60.3 25.6 %all-gather.12.cloned.1.call-done = bf16[256,2048]{1,0:T(8,128)(2,1)} async-done(((bf16[256,512]{1,0:T(8,128)(2,1)}), bf16[256,2048]{1,0:T(8,128)(2,1)}) %all-gather.12.cloned.1.call-update) | async-done | bytes 1048592 | tf_op jit(solution)/shard_map/all_gather | solution.py:82
  85.9 0.0 all-gather.14.cloned.1.call-update
  85.9 0.0 reduce-scatter.2.cloned.1.call-start
  86.0 88.5 %all-gather.10.cloned.1.call-done = bf16[2048,2048]{1,0:T(8,128)(2,1)} async-done(((bf16[2048,512]{1,0:T(8,128)(2,1)}), bf16[2048,2048]{1,0:T(8,128)(2,1)}) %all-gather.10.cloned.1.call-update) | async-done | bytes 8388624 | tf_op jit(solution)/shard_map/all_gather | solution.py:78
  174.5 4.7 %convolution_convert_fusion = bf16[128,2048]{1,0:T(8,128)(2,1)S(1)} fusion(bf16[2048,2048]{1,0:T(8,128)(2,1)} %all-gather.10.cloned.1.call-done, bf16[1,128,2048]{2,1,0:T(8,128)(2,1)S(1)} %all_gather.25, f32[2048]{0:T(1024)S(1)} %copy-done.2, f32[128]{0:T(128)S(1)} %add_rsqrt_fusion.1), kind=kOutput, calls=%fused_computation.5 | convolution fusion | flops 1075052544 | bytes 9445888 | tf_op jit(solution)/shard_map/dot_general | solution.py:79
  179.2 3.4 %collective-permute-start = (bf16[16,512]{1,0:T(8,128)(2,1)S(1)}, bf16[16,512]{1,0:T(8,128)(2,1)S(1)}, u32[]{:S(2)}, u32[]{:S(2)}) collective-permute-start(bf16[16,512]{1,0:T(8,128)(2,1)S(1)} %slice.154), channel_id=1, source_target_pairs={{0,8},{8,16},{16,24},{1,9},{9,17},{17,25},{2,10},{10,18},{18,26},{... | collective-permute-start | bytes 49160 | tf_op jit(solution)/shard_map/ppermute | solution.py:16
  182.6 0.2 negate_log-plus-one_fusion
  182.8 0.1 reshape.233
  182.9 0.1 reshape.232
  183.0 0.1 reshape.234
  183.2 0.2 fusion.46
  183.4 0.2 exponential_multiply_fusion
  183.6 0.6 fusion.41
  184.2 0.5 while.26
  184.3 0.2 bitcast_add_fusion.2
  184.5 0.2 bitcast_add_fusion.2
  184.8 9.1 %all-gather.2 = bf16[4,4,128]{2,1,0:T(4,128)(2,1)S(1)} all-gather(bf16[1,4,128]{2,1,0:T(4,128)(2,1)S(1)} %fusion.57), channel_id=2, replica_groups=mesh['sp'=4,'fs'=4,'tp'=2] {'sp'}, dimensions={0}, use_global_device_ids=true | all-gather | bytes 5120 | tf_op jit(solution)/shard_map/all_gather | solution.py:22
  193.8 14.9 %all-gather.1 = bf16[16,128,128]{2,1,0:T(8,128)(2,1)S(1)} all-gather(bf16[4,128,128]{2,1,0:T(8,128)(2,1)S(1)} %convert_element_type.223), channel_id=3, replica_groups=mesh['sp'=4,'fs'=4,'tp'=2] {'sp'}, dimensions={0}, use_global_device_ids=true | all-gather | bytes 655360 | tf_op jit(solution)/shard_map/all_gather | solution.py:22
  208.7 0.5 convolution_multiply_fusion
  209.3 0.3 fusion.54
  209.6 0.8 multiply_reduce_fusion
  210.4 0.3 copy.117
  210.7 0.3 reshape.244
  211.0 0.1 rsqrt.21
  211.1 0.1 fusion.39
  211.3 0.5 fusion.61
  211.8 0.5 convolution_bitcast_fusion
  212.3 0.1 copy.105
  212.4 0.0 copy-done.4
  212.4 0.1 fusion.40
  212.6 16.2 %all-gather.14.cloned.1.call-done = bf16[1024,2048]{1,0:T(8,128)(2,1)} async-done(((bf16[256,2048]{1,0:T(8,128)(2,1)}), bf16[1024,2048]{1,0:T(8,128)(2,1)}) %all-gather.14.cloned.1.call-update) | async-done | bytes 4194320 | tf_op jit(solution)/shard_map/all_gather | solution.py:83
  228.8 3.7 %convolution_convert_fusion.1 = bf16[128,2048]{1,0:T(8,128)(2,1)} fusion(bf16[1024,2048]{1,0:T(8,128)(2,1)} %all-gather.14.cloned.1.call-done, bf16[128,512]{0,1:T(8,128)(2,1)S(1)} %fusion.39, bf16[128,512]{0,1:T(8,128)(2,1)S(1)} %fusion.40), kind=kOutput, calls=%fused_computation.6 | convolution fusion | flops 537657344 | bytes 4980736 | tf_op jit(solution)/shard_map/dot_general | solution.py:159
  232.5 0.0 reduce-scatter.2.cloned.1.call-update
  232.5 8.1 %reduce-scatter.2.cloned.1.call-done = bf16[64,2048]{1,0:T(8,128)(2,1)} async-done(((bf16[128,2048]{1,0:T(8,128)(2,1)}), bf16[64,2048]{1,0:T(8,128)(2,1)}) %reduce-scatter.2.cloned.1.call-update) | async-done | bytes 262160 | tf_op jit(solution)/shard_map/reduce_scatter | solution.py:158
  (46 shorter events, 0.4 us)
Async XLA Ops:
  6.5 205.2 %copy-start = (bf16[2,256,256]{2,1,0:T(8,128)(2,1)S(1)}, bf16[2,256,256]{2,1,0:T(8,128)(2,1)}, u32[]{:S(2)}) copy-start(bf16[2,256,256]{2,1,0:T(8,128)(2,1)} %param.23) | copy-start | bytes 786436
  6.5 51.1 %copy-start.5 = (f32[1,128,4]{1,2,0:T(4,128)S(1)}, f32[1,128,4]{1,2,0:T(4,128)}, u32[]{:S(2)}) copy-start(f32[1,128,4]{1,2,0:T(4,128)} %param.26) | copy-start | bytes 6148
  6.5 51.3 %copy-start.1 = (bf16[1,64,2048]{2,1,0:T(8,128)(2,1)S(1)}, bf16[1,64,2048]{2,1,0:T(8,128)(2,1)}, u32[]{:S(2)}) copy-start(bf16[1,64,2048]{2,1,0:T(8,128)(2,1)} %param.17) | copy-start | bytes 786436
  6.5 53.8 %copy-start.6 = (f32[512]{0:T(512)S(1)}, f32[512]{0:T(512)}, u32[]{:S(2)}) copy-start(f32[512]{0:T(512)} %param.25) | copy-start | bytes 6148
  6.5 51.0 %all-gather.8.cloned.1.call-start = ((), (), s32[]{:S(2)}) async-start(), calls=%async_computation.1 | async-start | bytes 2621440 | tf_op jit(solution)/shard_map/all_gather | solution.py:77
  6.6 167.9 %copy-start.2 = (f32[2048]{0:T(1024)S(1)}, f32[2048]{0:T(1024)}, u32[]{:S(2)}) copy-start(f32[2048]{0:T(1024)} %param.18) | copy-start | bytes 24580
  8.9 77.0 %all-gather.12.cloned.1.call-start = ((), (), s32[]{:S(2)}) async-start(), calls=%async_computation.3 | async-start | bytes 1310720 | tf_op jit(solution)/shard_map/all_gather | solution.py:82
  10.9 163.6 %all-gather.10.cloned.1.call-start = ((), (), s32[]{:S(2)}) async-start(), calls=%async_computation.2 | async-start | bytes 10485760 | tf_op jit(solution)/shard_map/all_gather | solution.py:78
  57.5 171.3 %all-gather.14.cloned.1.call-start = ((), (), s32[]{:S(2)}) async-start(), calls=%async_computation.4 | async-start | bytes 5242880 | tf_op jit(solution)/shard_map/all_gather | solution.py:83
  85.9 154.7 %reduce-scatter.2.cloned.1.call-start = ((), (), s32[]{:S(2)}) async-start(), calls=%async_computation.5 | async-start | bytes 786432 | tf_op jit(solution)/shard_map/reduce_scatter | solution.py:158
  179.2 32.0 %collective-permute-start = (bf16[16,512]{1,0:T(8,128)(2,1)S(1)}, bf16[16,512]{1,0:T(8,128)(2,1)S(1)}, u32[]{:S(2)}, u32[]{:S(2)}) collective-permute-start(bf16[16,512]{1,0:T(8,128)(2,1)S(1)} %slice.154), channel_id=1, source_target_pairs={{0,8},{8,16},{16,24},{1,9},{9,17},{17,25},{2,10},{10,18},{18,26},{... | collective-permute-start | bytes 49160 | tf_op jit(solution)/shard_map/ppermute | solution.py:16
  208.7 2.4 copy-start.3
  211.8 0.7 copy-start.4
Sparse Core Ops, SparseCore 0:
  9.1 48.4 all-gather.7
  59.1 26.7 all-gather.11
  87.7 86.7 all-gather.9
  176.2 52.5 all-gather.13
  232.7 7.9 reduce-scatter.1
where the time goes:
time: 247 us
  waiting for transfers between devices  185 us (75%)
  blocking collectives  26.1 us (11%)
  between operations  13.5 us (5%)
  matrix products  11.1 us (4%)
  other arithmetic  5.86 us (2%)
  starting transfers between devices  3.58 us (1%)
    all_gather x1, waiting for transfers between devices, body(): full_input = lax.all_gather(column_part, 'fs', axis=1, tiled=True)  88.5 us
    all_gather x1, waiting for transfers between devices, body(): column_part = lax.all_gather(own_slice, 'sp', axis=0, tiled=True)  46.6 us
    all_gather x1, waiting for transfers between devices, body(): row_part = lax.all_gather(own_rows, 'sp', axis=1, tiled=True)  25.6 us
    all_gather x2, blocking collectives, entering(): lax.all_gather(a.astype(kind), axis)  23.9 us
    all_gather x1, waiting for transfers between devices, body(): out_full = lax.all_gather(row_part, 'fs', axis=0, tiled=True)  16.2 us
    reduce_scatter x1, waiting for transfers between devices, body(): lax.psum_scatter(jnp.dot(mixed_rows, out_full, preferred_element_type=jnp...  8.08 us
  transfers between devices with their start and end apart: 6, of which 5 were waited for; matrix products, arithmetic and copies ran while one was open for 5% of the time, Pallas kernels for 0%

commit v1 on v0

--- a/solution.py
+++ b/solution.py
@@ -1,6 +1,10 @@
+import functools
+
 import jax
 import jax.numpy as jnp
 from jax import lax
+from jax.experimental import pallas as pl
+from jax.experimental.pallas import tpu as pltpu
 from jax.sharding import PartitionSpec as P
 
 BLOCK = 64
@@ -164,6 +168,351 @@
     return summed[None]
 
 
+F32 = jnp.float32
+BF16 = jnp.bfloat16
+NT = (((1,), (1,)), ((), ()))
+TN = (((0,), (0,)), ((), ()))
+
+
+def layer_kernel(
+    n_sp, n_fs, n_tp,
+    tok, gain, w_pool, w_query, w_forget, w_value, maps, scale, low, spike, hgain, w_po, w_ro,
+    out,
+    wbuf, tbuf, nbuf, sbuf, proj, pool_g, rec_g, part, dbuf, summed, obuf,
+    wz_s, wz_r, wf_s, wf_r, tz_s, tz_r, td_s, td_r, ss_s, ss_r, pg_s, pg_r, rg_s, rg_r, d_s, d_r, o_s, o_r,
+):
+    s = lax.axis_index("sp")
+    f = lax.axis_index("fs")
+    t = lax.axis_index("tp")
+    rows = tok.shape[0]
+    depth = w_pool.shape[0]
+    width = w_pool.shape[1] // n_sp
+    piece = depth // n_fs
+    length = n_sp * n_tp * rows
+    weights = (w_pool, w_query, w_forget, w_value)
+
+    def at(ds=0, df=0):
+        return {"sp": lax.rem(s + ds, n_sp), "fs": lax.rem(f + df, n_fs), "tp": t}
+
+    other = {"sp": s, "fs": f, "tp": 1 - t}
+
+    def remote(src, dst, ssem, rsem, dev):
+        return pltpu.make_async_remote_copy(
+            src_ref=src, dst_ref=dst, send_sem=ssem, recv_sem=rsem,
+            device_id=dev, device_id_type=pl.DeviceIdType.MESH,
+        )
+
+    barrier = pltpu.get_barrier_semaphore()
+    partners = [at(ds=d) for d in range(1, n_sp)] + [at(df=e) for e in range(1, n_fs)] + [other]
+    for dev in partners:
+        pl.semaphore_signal(barrier, inc=1, device_id=dev, device_id_type=pl.DeviceIdType.MESH)
+    pl.semaphore_wait(barrier, len(partners))
+
+    def weight_copy(d, m):
+        dest = lax.rem(s + d, n_sp)
+        src = weights[m].at[pl.ds(pl.multiple_of(f * piece, piece), piece), pl.ds(pl.multiple_of(dest * width, width), width)]
+        dst = wbuf.at[pl.ds(pl.multiple_of(s * depth + f * piece, piece), piece), pl.ds(m * width, width)]
+        return remote(src, dst, wz_s.at[d - 1, m], wz_r.at[d - 1, m], at(ds=d))
+
+    def weight_pass(d, e):
+        origin = lax.rem(s - d + n_sp, n_sp)
+        view = wbuf.at[pl.ds(pl.multiple_of(origin * depth + f * piece, piece), piece), :]
+        return remote(view, view, wf_s.at[d - 1, e - 1], wf_r.at[d - 1, e - 1], at(df=e))
+
+    def weight_received(d, e):
+        origin = lax.rem(s - d + n_sp, n_sp)
+        giver = lax.rem(f - e + n_fs, n_fs)
+        view = wbuf.at[pl.ds(pl.multiple_of(origin * depth + giver * piece, piece), piece), :]
+        return remote(view, view, wf_s.at[d - 1, e - 1], wf_r.at[d - 1, e - 1], at(df=e))
+
+    def weight_arrival(d, m):
+        origin = lax.rem(s - d + n_sp, n_sp)
+        dst = wbuf.at[pl.ds(pl.multiple_of(origin * depth + f * piece, piece), piece), pl.ds(m * width, width)]
+        return remote(dst, dst, wz_s.at[d - 1, m], wz_r.at[d - 1, m], at(ds=d))
+
+    def spike_copy(d):
+        dest = lax.rem(s + d, n_sp)
+        return remote(spike.at[dest], sbuf.at[s], ss_s.at[d - 1], ss_r.at[d - 1], at(ds=d))
+
+    def line(own, slots, send_sems, recv_sems):
+        def sending(way, k):
+            step = 1 - 2 * way
+            origin = s - step * k
+            dst = slots(origin)
+            src = own if k == 0 else dst
+            return remote(src, dst, send_sems.at[way, k], recv_sems.at[way, k], at(ds=step + n_sp))
+
+        def arriving(way, k):
+            step = 1 - 2 * way
+            dst = slots(s - step * (k + 1))
+            return remote(dst, dst, send_sems.at[way, k], recv_sems.at[way, k], at(ds=step + n_sp))
+
+        def can_send(way, k):
+            if way == 0:
+                return jnp.logical_and(s - k >= 0, s + 1 < n_sp)
+            return jnp.logical_and(s + k < n_sp, s - 1 >= 0)
+
+        def will_arrive(way, k):
+            return s - (k + 1) >= 0 if way == 0 else s + (k + 1) < n_sp
+
+        return sending, arriving, can_send, will_arrive
+
+    def hop_start(parts, k):
+        sending, _, can_send, _ = parts
+        for way in (0, 1):
+            @pl.when(can_send(way, k))
+            def _(way=way):
+                sending(way, k).start()
+
+    def hop_finish(parts):
+        sending, _, can_send, _ = parts
+        for k in range(n_sp - 1):
+            for way in (0, 1):
+                @pl.when(can_send(way, k))
+                def _(way=way, k=k):
+                    sending(way, k).wait_send()
+
+    for d in (1, 3, 2) if n_sp == 4 else range(1, n_sp):
+        for m in range(4):
+            weight_copy(d, m).start()
+    tokens_line = line(tok, lambda o: tbuf.at[o, t], tz_s, tz_r)
+    hop_start(tokens_line, 0)
+    own_pass = remote(tok, tbuf.at[s, t], td_s.at[s], td_r.at[s], other)
+    own_pass.start()
+    for d in range(1, n_sp):
+        spike_copy(d).start()
+
+    def core_pass(origin):
+        view = tbuf.at[origin, t]
+        return remote(view, view, td_s.at[origin], td_r.at[origin], other)
+
+    def core_arrival(origin):
+        view = tbuf.at[origin, 1 - t]
+        return remote(view, view, td_s.at[origin], td_r.at[origin], other)
+
+    gain_row = gain[...]
+
+    def normalise(values, origin, core):
+        x = values.astype(F32)
+        y = x * lax.rsqrt(jnp.mean(x * x, axis=-1, keepdims=True) + EPSILON) * gain_row
+        nbuf[origin, core] = y.astype(BF16)
+
+    for m in range(4):
+        wbuf[pl.ds(pl.multiple_of(s * depth, depth), depth), m * width:(m + 1) * width] = weights[m][
+            :, pl.ds(pl.multiple_of(s * width, width), width)
+        ]
+    sbuf[s] = spike[s]
+    normalise(tok[...], s, t)
+
+    order = (1, 3, 2) if n_sp == 4 else tuple(range(1, n_sp))
+    for k in range(n_sp - 1):
+        for way in (0, 1):
+            @pl.when(tokens_line[3](way, k))
+            def _(way=way, k=k):
+                tokens_line[1](way, k).wait_recv()
+                if k + 1 < n_sp - 1:
+                    @pl.when(tokens_line[2](way, k + 1))
+                    def _():
+                        tokens_line[0](way, k + 1).start()
+                core_pass(s - (1 - 2 * way) * (k + 1)).start()
+        d = order[k]
+        for m in range(4):
+            weight_arrival(d, m).wait_recv()
+        for e in range(1, n_fs):
+            weight_pass(d, e).start()
+        for way in (0, 1):
+            @pl.when(tokens_line[3](way, k))
+            def _(way=way, k=k):
+                origin = s - (1 - 2 * way) * (k + 1)
+                normalise(tbuf[origin, t], origin, t)
+
+    @pl.loop(0, n_sp)
+    def _(origin):
+        core_arrival(origin).wait_recv()
+        normalise(tbuf[origin, 1 - t], origin, 1 - t)
+
+    for d in order:
+        for e in range(1, n_fs):
+            weight_received(d, e).wait_recv()
+    for d in range(1, n_sp):
+        dst = sbuf.at[lax.rem(s - d + n_sp, n_sp)]
+        remote(dst, dst, ss_s.at[d - 1], ss_r.at[d - 1], at(ds=d)).wait_recv()
+
+    @pl.loop(0, n_sp)
+    def _(origin):
+        x = nbuf[origin].reshape(n_tp * rows, nbuf.shape[3])
+        proj[origin] = jnp.dot(x, wbuf[...], preferred_element_type=F32).astype(BF16)
+
+    projected = proj[...].reshape(length, 4 * width)
+    x = projected[:, :width].astype(F32)
+    group_size = maps.shape[1]
+    groups = maps.shape[0]
+    share = group_size // width
+    group = t * groups + s // share
+    position = lax.broadcasted_iota(jnp.int32, (length, width), 0)
+    total = x
+    window_sum = x
+    window = jnp.int32(2)
+    for g in range(n_tp * groups):
+        reach = 2 ** g
+        total = total + jnp.concatenate([jnp.zeros((reach, width), F32), total[: length - reach]], axis=0)
+        window_sum = total if g == 0 else jnp.where(group == g, total, window_sum)
+    for g in range(1, n_tp * groups):
+        window = jnp.where(group == g, 2 ** (g + 1), window)
+    counts = jnp.minimum(position + 1, window).astype(F32)
+    pool_g[s] = (window_sum / counts - x).astype(BF16)
+    pool_line = line(pool_g.at[s], lambda o: pool_g.at[o], pg_s, pg_r)
+    hop_start(pool_line, 0)
+
+    lows = low[s]
+    tri_r = lax.broadcasted_iota(jnp.int32, (BLOCK, BLOCK), 0)
+    tri_c = lax.broadcasted_iota(jnp.int32, (BLOCK, BLOCK), 1)
+    causal = tri_r >= tri_c
+    tri = causal.astype(F32)
+    gate_low = jax.nn.sigmoid(-lows)
+    state = jnp.zeros((width, width), F32)
+    per_origin = length // n_sp
+    columns = [jnp.transpose(sbuf[o])[:, :1] for o in range(n_sp)]
+    for b in range(length // BLOCK):
+        lo = b * BLOCK
+        here = slice(lo, lo + BLOCK)
+        q = projected[here, width:2 * width].astype(F32)
+        logit = projected[here, 2 * width:3 * width].astype(F32)
+        v = projected[here, 3 * width:]
+        reader = q * jax.nn.sigmoid(q)
+        key = gate_low * jax.nn.sigmoid(-logit)
+        off = lo % per_origin
+        logs = jnp.log1p(-key) + columns[lo // per_origin][off:off + BLOCK]
+        inner = jnp.dot(tri, logs, preferred_element_type=F32, precision=HIGHEST)
+        read_scaled = (reader * jnp.exp(inner)).astype(BF16)
+        key_scaled = (key * jnp.exp(-inner)).astype(BF16)
+        scores = lax.dot_general(read_scaled, key_scaled, NT, preferred_element_type=F32)
+        scores = jnp.where(causal, scores, 0.0).astype(BF16)
+        read = jnp.dot(scores, v, preferred_element_type=F32)
+        read = read + lax.dot_general(read_scaled, state.astype(BF16), NT, preferred_element_type=F32)
+        closing = inner[BLOCK - 1:]
+        key_tail = (key * jnp.exp(closing - inner)).astype(BF16)
+        state = jnp.exp(closing) * state + lax.dot_general(v, key_tail, TN, preferred_element_type=F32)
+        rec = read * lax.rsqrt(jnp.mean(read * read, axis=-1, keepdims=True) + EPSILON) * hgain[s]
+        rec_g[s, lo:lo + BLOCK] = rec.astype(BF16)
+    rec_line = line(rec_g.at[s], lambda o: rec_g.at[o], rg_s, rg_r)
+    hop_start(rec_line, 0)
+
+    for k in range(n_sp - 1):
+        for parts in (pool_line, rec_line):
+            for way in (0, 1):
+                @pl.when(parts[3](way, k))
+                def _(way=way, k=k, parts=parts):
+                    parts[1](way, k).wait_recv()
+                    if k + 1 < n_sp - 1:
+                        @pl.when(parts[2](way, k + 1))
+                        def _():
+                            parts[0](way, k + 1).start()
+
+    strip = n_tp * rows
+    @pl.loop(0, n_sp)
+    def _(o):
+        here = pl.ds(pl.multiple_of(o * strip, strip), strip)
+        mixed_row = []
+        for g in range(groups):
+            diff = jnp.concatenate([pool_g[g * share + c, here] for c in range(share)], axis=1)
+            mapped = jnp.dot(diff, maps[g], preferred_element_type=F32)
+            mixed_row.append((mapped * scale[:, g * group_size:(g + 1) * group_size]).astype(BF16))
+        acc = jnp.dot(jnp.concatenate(mixed_row, axis=1), w_po[...], preferred_element_type=F32)
+        recs = jnp.concatenate([rec_g[c, here] for c in range(n_sp)], axis=1)
+        acc = acc + jnp.dot(recs, w_ro[...], preferred_element_type=F32)
+        acc = acc.astype(BF16)
+        for core in range(n_tp):
+            part[core, o] = acc[core * rows:(core + 1) * rows]
+
+    across = remote(part.at[1 - t], dbuf, d_s, d_r, other)
+    across.start()
+    across.wait_recv()
+    summed[...] = (part[t].astype(F32) + dbuf[...].astype(F32)).astype(BF16)
+
+    def out_copy(d):
+        dest = lax.rem(s + d, n_sp)
+        return remote(summed.at[dest], obuf.at[s], o_s.at[d - 1], o_r.at[d - 1], at(ds=d))
+
+    for d in order:
+        out_copy(d).start()
+    obuf[s] = summed[s]
+    for d in order:
+        dst = obuf.at[lax.rem(s - d + n_sp, n_sp)]
+        remote(dst, dst, o_s.at[d - 1], o_r.at[d - 1], at(ds=d)).wait_recv()
+    cols = w_po.shape[1]
+    for o in range(n_sp):
+        out[:, o * cols:(o + 1) * cols] = obuf[o]
+
+    for d in range(1, n_sp):
+        for m in range(4):
+            weight_copy(d, m).wait_send()
+        for e in range(1, n_fs):
+            weight_pass(d, e).wait_send()
+        spike_copy(d).wait_send()
+        out_copy(d).wait_send()
+    hop_finish(tokens_line)
+    hop_finish(pool_line)
+    hop_finish(rec_line)
+    own_pass.wait_send()
+    for k in range(n_sp - 1):
+        for way in (0, 1):
+            @pl.when(tokens_line[3](way, k))
+            def _(way=way, k=k):
+                core_pass(s - (1 - 2 * way) * (k + 1)).wait_send()
+    across.wait_send()
+
+
+def head_body(sizes, *args):
+    (tokens, gain, w_pool, w_query, w_forget, w_value, maps, scale, low, spike, hgain, w_po, w_ro) = args
+    n_sp, n_fs, n_tp = sizes
+    tok = tokens[0]
+    rows, features = tok.shape
+    width = w_pool.shape[1] // n_sp
+    length = n_sp * n_tp * rows
+    cols = w_po.shape[1]
+    spikes = jnp.broadcast_to(spike[0].T[:, None, :], (spike.shape[2], 8, spike.shape[1]))
+    dma = pltpu.SemaphoreType.DMA
+    whole = pl.BlockSpec(memory_space=pltpu.VMEM)
+    hop = (2, n_sp - 1)
+    result = pl.pallas_call(
+        functools.partial(layer_kernel, n_sp, n_fs, n_tp),
+        out_shape=jax.ShapeDtypeStruct((rows, n_sp * cols), BF16),
+        in_specs=[whole] * 13,
+        out_specs=whole,
+        scratch_shapes=[
+            pltpu.VMEM((features, 4 * width), BF16),
+            pltpu.VMEM((n_sp, n_tp, rows, features), BF16),
+            pltpu.VMEM((n_sp, n_tp, rows, features), BF16),
+            pltpu.VMEM((n_sp, 8, spike.shape[1]), F32),
+            pltpu.VMEM((n_sp, n_tp * rows, 4 * width), BF16),
+            pltpu.VMEM((n_sp, length, width), BF16),
+            pltpu.VMEM((n_sp, length, width), BF16),
+            pltpu.VMEM((n_tp, n_sp, rows, cols), BF16),
+            pltpu.VMEM((n_sp, rows, cols), BF16),
+            pltpu.VMEM((n_sp, rows, cols), BF16),
+            pltpu.VMEM((n_sp, rows, cols), BF16),
+            dma((n_sp - 1, 4)), dma((n_sp - 1, 4)),
+            dma((n_sp - 1, n_fs - 1)), dma((n_sp - 1, n_fs - 1)),
+            dma(hop), dma(hop),
+            dma((n_sp,)), dma((n_sp,)),
+            dma((n_sp - 1,)), dma((n_sp - 1,)),
+            dma(hop), dma(hop),
+            dma(hop), dma(hop),
+            dma, dma,
+            dma((n_sp - 1,)), dma((n_sp - 1,)),
+        ],
+        compiler_params=pltpu.CompilerParams(
+            collective_id=0, has_side_effects=True, vmem_limit_bytes=56 * 1024 * 1024
+        ),
+        name="layer",
+    )(
+        tok, gain[None], w_pool, w_query, w_forget, w_value, maps, scale[None],
+        low.reshape(n_sp, 1, width), spikes, hgain.reshape(n_sp, 1, width), w_po, w_ro,
+    )
+    return result[None]
+
+
 def solution(mesh):
     placed = (
         P("fs", ("sp", "tp"), None),
@@ -180,6 +529,15 @@
         P("tp", "sp"),
         P("tp", "sp"),
     )
+    sizes = (mesh.shape["sp"], mesh.shape["fs"], mesh.shape["tp"])
+
+    def one(*args):
+        maps, spike = args[6], args[9]
+        width = args[2].shape[1] // sizes[0]
+        fits = spike.shape[2] == sizes[0] and sizes[2] == 2 and width % 128 == 0
+        fits = fits and args[3].shape[1] == args[2].shape[1] and maps.shape[1] % width == 0
+        return head_body(sizes, *args) if fits else body(*args)
+
     return jax.shard_map(
-        body, mesh=mesh, in_specs=placed, out_specs=P("fs", ("sp", "tp"), None), check_vma=False
-    )
+        one, mesh=mesh, in_specs=placed, out_specs=P("fs", ("sp", "tp"), None), check_vma=False
+    )

time: 247 us -> 77.2 us (0.31)
  waiting for transfers between devices: 185 us -> 0 us
  Pallas kernels: 0 us -> 73 us
  blocking collectives: 26.1 us -> 0 us
  between operations: 13.5 us -> 0.01 us
  matrix products: 11.1 us -> 0 us
  other arithmetic: 5.86 us -> 0 us
  starting transfers between devices: 3.58 us -> 0 us
    all_gather x4 -> x0, waiting for transfers between devices: 177 us -> none  [the longest x1 88.5 us: body(): full_input = lax.all_gather(column_part, 'fs', axis=1, tiled=True)]
    pallas_call x0 -> x1, Pallas kernels: none -> 73 us  [head_body(): pl.pallas_call(functools.partial(layer_kernel, n_sp, n_fs, n_tp), out_sha...]
    all_gather x3 -> x0, blocking collectives: 26.1 us -> none  [the longest x2 23.9 us: entering(): lax.all_gather(a.astype(kind), axis)]
    dot_general x7 -> x0, matrix products: 11.1 us -> none  [the longest x1 4.68 us: body(): projected = jnp.dot(normed, full_input, preferred_element_type=jnp.float32)]
    reduce_scatter x1 -> x0, waiting for transfers between devices: 8.08 us -> none  [body(): lax.psum_scatter(jnp.dot(mixed_rows, out_full, preferred_element_type=jnp...]
    concatenate x2 -> x0, other arithmetic: 4.15 us -> none  [the longest x1 2.31 us: body(): jnp.concatenate([pooling_input_weight, query_weight, forget_weight, value...]
    ppermute x1 -> x0, starting transfers between devices: 3.39 us -> none  [shifted(): lax.ppermute(value, axis, [(source, source + steps) for source in range(f...]
  transfers between devices with their start and end apart: 6 -> 0, of which waited for: 5 -> 0; matrix products, arithmetic and copies ran while one was open for 5% -> 0% of each run, Pallas kernels for 0% -> 0%
where the time goes in v1:
time: 77.2 us; the launch traced here: 76 us
  Pallas kernels  73 us (95%)
  local copies, waits for them, and re-layouts  2.96 us (4%)
    pallas_call x1, Pallas kernels, head_body(): pl.pallas_call(functools.partial(layer_kernel, n_sp, n_fs, n_tp), out_sha...  73 us
    unnamed x3, local copies, waits for them, and re-layouts  2.35 us

profile of v1, /device:TPU:0, one launch (start us, length us, event | category | flops | bytes accessed | tf_op | source)
XLA Modules:
  0.0 76.0 jit_solution(16614216100563509335)
XLA Ops:
  0.0 0.0 copy-start
  0.0 0.7 copy-done
  0.7 0.6 broadcast_in_dim.17.spike
  1.3 73.0 %layer.1 = bf16[64,2048]{1,0:T(8,128)(2,1)} custom-call(bf16[64,2048]{1,0:T(8,128)(2,1)} %bitcast.10, f32[1,2048]{1,0:T(1,128)} %bitcast.11, bf16[512,512]{1,0:T(8,128)(2,1)} %w_pool.1, bf16[512,512]{1,0:T(8,128)(2,1)} %w_query.1, bf16[512,512]{1,0:T(8,128)(2,1)} %w_forget.1, bf16[512,512]{1,0:T(8,128)(2,1)} %w_value.1, bf16[2,256,256]{2,1,0:T(8,128)(2,1)} %maps.1, ...), custom_call_target="tpu_custom_call" | custom-call | tf_op jit(solution)/shard_map/layer/pallas_call | solution.py:478
  74.3 1.7 %copy.15 = bf16[1,64,2048]{2,1,0:T(8,128)(2,1)} copy(bf16[1,64,2048]{2,1,0:T(8,128)(2,1)} %bitcast.9) | data formatting | bytes 524288
Async XLA Ops:
  0.0 0.7 copy-start

commit v2 on v1

--- a/solution.py
+++ b/solution.py
@@ -305,21 +305,22 @@
     normalise(tok[...], s, t)
 
     order = (1, 3, 2) if n_sp == 4 else tuple(range(1, n_sp))
+    for d in order:
+        for m in range(4):
+            weight_arrival(d, m).wait_recv()
+        for e in range(1, n_fs):
+            weight_pass(d, e).start()
     for k in range(n_sp - 1):
         for way in (0, 1):
             @pl.when(tokens_line[3](way, k))
             def _(way=way, k=k):
+                origin = s - (1 - 2 * way) * (k + 1)
                 tokens_line[1](way, k).wait_recv()
                 if k + 1 < n_sp - 1:
                     @pl.when(tokens_line[2](way, k + 1))
                     def _():
                         tokens_line[0](way, k + 1).start()
-                core_pass(s - (1 - 2 * way) * (k + 1)).start()
-        d = order[k]
-        for m in range(4):
-            weight_arrival(d, m).wait_recv()
-        for e in range(1, n_fs):
-            weight_pass(d, e).start()
+                core_pass(origin).start()
         for way in (0, 1):
             @pl.when(tokens_line[3](way, k))
             def _(way=way, k=k):
@@ -338,10 +339,12 @@
         dst = sbuf.at[lax.rem(s - d + n_sp, n_sp)]
         remote(dst, dst, ss_s.at[d - 1], ss_r.at[d - 1], at(ds=d)).wait_recv()
 
-    @pl.loop(0, n_sp)
-    def _(origin):
-        x = nbuf[origin].reshape(n_tp * rows, nbuf.shape[3])
-        proj[origin] = jnp.dot(x, wbuf[...], preferred_element_type=F32).astype(BF16)
+    tall = max(1, n_sp // 2)
+    @pl.loop(0, n_sp // tall)
+    def _(i):
+        x = nbuf[pl.ds(i * tall, tall)].reshape(tall * n_tp * rows, nbuf.shape[3])
+        y = jnp.dot(x, wbuf[...], preferred_element_type=F32).astype(BF16)
+        proj[pl.ds(i * tall, tall)] = y.reshape(tall, n_tp * rows, 4 * width)
 
     projected = proj[...].reshape(length, 4 * width)
     x = projected[:, :width].astype(F32)
@@ -395,24 +398,53 @@
         state = jnp.exp(closing) * state + lax.dot_general(v, key_tail, TN, preferred_element_type=F32)
         rec = read * lax.rsqrt(jnp.mean(read * read, axis=-1, keepdims=True) + EPSILON) * hgain[s]
         rec_g[s, lo:lo + BLOCK] = rec.astype(BF16)
-    rec_line = line(rec_g.at[s], lambda o: rec_g.at[o], rg_s, rg_r)
-    hop_start(rec_line, 0)
+    strip = n_tp * rows
+    strips = (0, 3, 1, 2) if n_sp == 4 else tuple(range(n_sp))
+
+    def strip_line(p):
+        here = pl.ds(p * strip, strip)
+        return line(rec_g.at[s, here], lambda o: rec_g.at[o, here], rg_s.at[p], rg_r.at[p])
+
+    rec_lines = [strip_line(p) for p in range(n_sp)]
+    for p in strips:
+        hop_start(rec_lines[p], 0)
+
+    def relay(parts, k):
+        for way in (0, 1):
+            @pl.when(parts[3](way, k))
+            def _(way=way):
+                parts[1](way, k).wait_recv()
+                if k + 1 < n_sp - 1:
+                    @pl.when(parts[2](way, k + 1))
+                    def _():
+                        parts[0](way, k + 1).start()
+
+    def across(p):
+        return remote(part.at[1 - t, p], dbuf.at[p], d_s.at[p], d_r.at[p], other)
+
+    def out_copy(p):
+        return remote(summed.at[p], obuf.at[s], o_s.at[p], o_r.at[s], {"sp": p, "fs": f, "tp": t})
+
+    def settle(p):
+        across(p).wait_recv()
+        summed[p] = (part[t, p].astype(F32) + dbuf[p].astype(F32)).astype(BF16)
+
+        @pl.when(s != p)
+        def _():
+            out_copy(p).start()
+
+        @pl.when(s == p)
+        def _():
+            obuf[p] = summed[p]
 
     for k in range(n_sp - 1):
-        for parts in (pool_line, rec_line):
-            for way in (0, 1):
-                @pl.when(parts[3](way, k))
-                def _(way=way, k=k, parts=parts):
-                    parts[1](way, k).wait_recv()
-                    if k + 1 < n_sp - 1:
-                        @pl.when(parts[2](way, k + 1))
-                        def _():
-                            parts[0](way, k + 1).start()
-
-    strip = n_tp * rows
-    @pl.loop(0, n_sp)
-    def _(o):
-        here = pl.ds(pl.multiple_of(o * strip, strip), strip)
+        relay(pool_line, k)
+        if k < n_sp - 2:
+            for p in strips:
+                relay(rec_lines[p], k)
+
+    def project(p):
+        here = slice(p * strip, (p + 1) * strip)
         mixed_row = []
         for g in range(groups):
             diff = jnp.concatenate([pool_g[g * share + c, here] for c in range(share)], axis=1)
@@ -423,23 +455,22 @@
         acc = acc + jnp.dot(recs, w_ro[...], preferred_element_type=F32)
         acc = acc.astype(BF16)
         for core in range(n_tp):
-            part[core, o] = acc[core * rows:(core + 1) * rows]
-
-    across = remote(part.at[1 - t], dbuf, d_s, d_r, other)
-    across.start()
-    across.wait_recv()
-    summed[...] = (part[t].astype(F32) + dbuf[...].astype(F32)).astype(BF16)
-
-    def out_copy(d):
-        dest = lax.rem(s + d, n_sp)
-        return remote(summed.at[dest], obuf.at[s], o_s.at[d - 1], o_r.at[d - 1], at(ds=d))
+            part[core, p] = acc[core * rows:(core + 1) * rows]
+        across(p).start()
+
+    before = None
+    for p in strips:
+        relay(rec_lines[p], n_sp - 2)
+        project(p)
+        if before is not None:
+            settle(before)
+        before = p
+    settle(before)
 
     for d in order:
-        out_copy(d).start()
-    obuf[s] = summed[s]
-    for d in order:
-        dst = obuf.at[lax.rem(s - d + n_sp, n_sp)]
-        remote(dst, dst, o_s.at[d - 1], o_r.at[d - 1], at(ds=d)).wait_recv()
+        origin = lax.rem(s + d, n_sp)
+        dst = obuf.at[origin]
+        remote(dst, dst, o_s.at[origin], o_r.at[origin], at(ds=d)).wait_recv()
     cols = w_po.shape[1]
     for o in range(n_sp):
         out[:, o * cols:(o + 1) * cols] = obuf[o]
@@ -450,17 +481,21 @@
         for e in range(1, n_fs):
             weight_pass(d, e).wait_send()
         spike_copy(d).wait_send()
-        out_copy(d).wait_send()
     hop_finish(tokens_line)
     hop_finish(pool_line)
-    hop_finish(rec_line)
+    for p in range(n_sp):
+        hop_finish(rec_lines[p])
+        across(p).wait_send()
+
+        @pl.when(s != p)
+        def _(p=p):
+            out_copy(p).wait_send()
     own_pass.wait_send()
     for k in range(n_sp - 1):
         for way in (0, 1):
             @pl.when(tokens_line[3](way, k))
             def _(way=way, k=k):
                 core_pass(s - (1 - 2 * way) * (k + 1)).wait_send()
-    across.wait_send()
 
 
 def head_body(sizes, *args):
@@ -498,9 +533,9 @@
             dma((n_sp,)), dma((n_sp,)),
             dma((n_sp - 1,)), dma((n_sp - 1,)),
             dma(hop), dma(hop),
-            dma(hop), dma(hop),
-            dma, dma,
-            dma((n_sp - 1,)), dma((n_sp - 1,)),
+            dma((n_sp,) + hop), dma((n_sp,) + hop),
+            dma((n_sp,)), dma((n_sp,)),
+            dma((n_sp,)), dma((n_sp,)),
         ],
         compiler_params=pltpu.CompilerParams(
             collective_id=0, has_side_effects=True, vmem_limit_bytes=56 * 1024 * 1024

time: 77.2 us -> 71.2 us (0.922); the launches traced: 76 us -> 71.1 us
  Pallas kernels: 73 us -> 68.1 us
    pallas_call x1, Pallas kernels: 73 us -> 68.1 us  [head_body(): pl.pallas_call(functools.partial(layer_kernel, n_sp, n_fs, n_tp), out_sha...]
where the time goes in v2:
time: 71.2 us; the launch traced here: 71.1 us
  Pallas kernels  68.1 us (96%)
  local copies, waits for them, and re-layouts  2.96 us (4%)
    pallas_call x1, Pallas kernels, head_body(): pl.pallas_call(functools.partial(layer_kernel, n_sp, n_fs, n_tp), out_sha...  68.1 us
    unnamed x3, local copies, waits for them, and re-layouts  2.35 us

profile of v2, /device:TPU:0, one launch (start us, length us, event | category | flops | bytes accessed | tf_op | source)
XLA Modules:
  0.0 71.1 jit_solution(4871893628677013588)
XLA Ops:
  0.0 0.0 copy-start
  0.0 0.7 copy-done
  0.7 0.6 broadcast_in_dim.17.spike
  1.3 68.1 %layer.1 = bf16[64,2048]{1,0:T(8,128)(2,1)} custom-call(bf16[64,2048]{1,0:T(8,128)(2,1)} %bitcast.10, f32[1,2048]{1,0:T(1,128)} %bitcast.11, bf16[512,512]{1,0:T(8,128)(2,1)} %w_pool.1, bf16[512,512]{1,0:T(8,128)(2,1)} %w_query.1, bf16[512,512]{1,0:T(8,128)(2,1)} %w_forget.1, bf16[512,512]{1,0:T(8,128)(2,1)} %w_value.1, bf16[2,256,256]{2,1,0:T(8,128)(2,1)} %maps.1, ...), custom_call_target="tpu_custom_call" | custom-call | tf_op jit(solution)/shard_map/layer/pallas_call | solution.py:513
  69.4 1.7 %copy.15 = bf16[1,64,2048]{2,1,0:T(8,128)(2,1)} copy(bf16[1,64,2048]{2,1,0:T(8,128)(2,1)} %bitcast.9) | data formatting | bytes 524288
Async XLA Ops:
  0.0 0.7 copy-start

commit v3 on v2

--- a/solution.py
+++ b/solution.py
@@ -310,10 +310,10 @@
             weight_arrival(d, m).wait_recv()
         for e in range(1, n_fs):
             weight_pass(d, e).start()
-    for k in range(n_sp - 1):
+    def token_hop(k):
         for way in (0, 1):
             @pl.when(tokens_line[3](way, k))
-            def _(way=way, k=k):
+            def _(way=way):
                 origin = s - (1 - 2 * way) * (k + 1)
                 tokens_line[1](way, k).wait_recv()
                 if k + 1 < n_sp - 1:
@@ -323,15 +323,18 @@
                 core_pass(origin).start()
         for way in (0, 1):
             @pl.when(tokens_line[3](way, k))
-            def _(way=way, k=k):
+            def _(way=way):
                 origin = s - (1 - 2 * way) * (k + 1)
                 normalise(tbuf[origin, t], origin, t)
 
-    @pl.loop(0, n_sp)
-    def _(origin):
+    def finish(origin):
         core_arrival(origin).wait_recv()
         normalise(tbuf[origin, 1 - t], origin, 1 - t)
-
+        x = nbuf[origin].reshape(n_tp * rows, nbuf.shape[3])
+        proj[origin] = jnp.dot(x, wbuf[...], preferred_element_type=F32).astype(BF16)
+
+    for k in range(n_sp - 2):
+        token_hop(k)
     for d in order:
         for e in range(1, n_fs):
             weight_received(d, e).wait_recv()
@@ -339,12 +342,21 @@
         dst = sbuf.at[lax.rem(s - d + n_sp, n_sp)]
         remote(dst, dst, ss_s.at[d - 1], ss_r.at[d - 1], at(ds=d)).wait_recv()
 
-    tall = max(1, n_sp // 2)
-    @pl.loop(0, n_sp // tall)
-    def _(i):
-        x = nbuf[pl.ds(i * tall, tall)].reshape(tall * n_tp * rows, nbuf.shape[3])
-        y = jnp.dot(x, wbuf[...], preferred_element_type=F32).astype(BF16)
-        proj[pl.ds(i * tall, tall)] = y.reshape(tall, n_tp * rows, 4 * width)
+    near_low = jnp.maximum(s - (n_sp - 2), 0)
+    near_high = jnp.minimum(s + (n_sp - 2), n_sp - 1)
+
+    @pl.loop(0, n_sp)
+    def _(origin):
+        @pl.when(jnp.logical_and(origin >= near_low, origin <= near_high))
+        def _():
+            finish(origin)
+
+    if n_sp > 1:
+        token_hop(n_sp - 2)
+    for way in (0, 1):
+        @pl.when(tokens_line[3](way, n_sp - 2))
+        def _(way=way):
+            finish(s - (1 - 2 * way) * (n_sp - 1))
 
     projected = proj[...].reshape(length, 4 * width)
     x = projected[:, :width].astype(F32)

time: 71.2 us -> 70.1 us (0.985)
  Pallas kernels: 68.1 us -> 66.9 us
    pallas_call x1, Pallas kernels: 68.1 us -> 66.9 us  [head_body(): pl.pallas_call(functools.partial(layer_kernel, n_sp, n_fs, n_tp), out_sha...]
where the time goes in v3:
time: 70.1 us; the launch traced here: 69.9 us
  Pallas kernels  66.9 us (95%)
  local copies, waits for them, and re-layouts  2.96 us (4%)
    pallas_call x1, Pallas kernels, head_body(): pl.pallas_call(functools.partial(layer_kernel, n_sp, n_fs, n_tp), out_sha...  66.9 us
    unnamed x3, local copies, waits for them, and re-layouts  2.35 us

profile of v3, /device:TPU:0, one launch (start us, length us, event | category | flops | bytes accessed | tf_op | source)
XLA Modules:
  0.0 69.9 jit_solution(4072434945456612581)
XLA Ops:
  0.0 0.0 copy-start
  0.0 0.7 copy-done
  0.7 0.6 broadcast_in_dim.17.spike
  1.3 66.9 %layer.1 = bf16[64,2048]{1,0:T(8,128)(2,1)} custom-call(bf16[64,2048]{1,0:T(8,128)(2,1)} %bitcast.10, f32[1,2048]{1,0:T(1,128)} %bitcast.11, bf16[512,512]{1,0:T(8,128)(2,1)} %w_pool.1, bf16[512,512]{1,0:T(8,128)(2,1)} %w_query.1, bf16[512,512]{1,0:T(8,128)(2,1)} %w_forget.1, bf16[512,512]{1,0:T(8,128)(2,1)} %w_value.1, bf16[2,256,256]{2,1,0:T(8,128)(2,1)} %maps.1, ...), custom_call_target="tpu_custom_call" | custom-call | tf_op jit(solution)/shard_map/layer/pallas_call | solution.py:525
  68.2 1.7 %copy.15 = bf16[1,64,2048]{2,1,0:T(8,128)(2,1)} copy(bf16[1,64,2048]{2,1,0:T(8,128)(2,1)} %bitcast.9) | data formatting | bytes 524288
Async XLA Ops:
  0.0 0.7 copy-start
